TPU v7x, 32 devices: a whole 2x2x4 slice. The times are simulated.
32 devices in a mesh: grp: 2 (over y), sp: 4 (over z), tp: 4 (over x, core).
Axes of the slice: x: 2, y: 2, z: 4, core: 2. Of those that a mesh axis runs over, the one named last changes fastest.
Arguments:
- conv_value: bfloat16 [4096, 1024], P(('grp', 'sp'), 'tp'), parts along dimension 0, may hold values from -6 to 6
- conv_gate: bfloat16 [4096, 1024], P(('grp', 'sp'), 'tp'), parts along dimension 0, may hold values from -6 to 6
- kernel: bfloat16 [31, 1024], P(None, 'tp'), may hold values from -4 to 4
- conv_bias: float32 [1024], P('tp'), may hold values from -3 to 3
- ln_gain: float32 [1024], P('tp'), may hold values from 0.1 to 1.9
- ln_bias: float32 [1024], P('tp'), may hold values from -3 to 3
- out_gain: float32 [1024], P('tp'), may hold values from 0.1 to 1.9
- out_weight: bfloat16 [1024, 2048], replicated, may hold values from -0.1875 to 0.1875
- residual: bfloat16 [4096, 2048], P(('grp', 'sp', 'tp')), parts along dimension 0, may hold values from -6 to 6
- moe_gain: float32 [2048], replicated, may hold values from 0.1 to 1.9
- expert_ids: int32 [4096, 2], P(('grp', 'sp', 'tp')), parts along dimension 0, may hold values from 0 to 15, as said below
- expert_weights: float32 [4096, 2], P(('grp', 'sp', 'tp')), parts along dimension 0, may hold values from 0.1 to 0.7
- w_gate: bfloat16 [16, 2048, 512], P(('sp', 'tp')), may hold values from -0.125 to 0.125
- w_up: bfloat16 [16, 2048, 512], P(('sp', 'tp')), may hold values from -0.125 to 0.125
- w_down: bfloat16 [16, 512, 2048], P(('sp', 'tp')), may hold values from -0.25 to 0.25
Outputs:
- layer_out: bfloat16 [4096, 2048], P(('grp', 'sp', 'tp')), parts along dimension 0
There are 2 independent parts, one for each index of `grp`. A program takes and returns all parts, laid end to end along the dimension named above; an argument that names none is the same for every part. Nothing has to cross between parts.
Inputs may be any that keep to these rules, and one draw needn't show every extreme that they name: `expert_ids`: each row names two different experts of one group (group = expert number // 4). Among the 128 rows of one device (aligned blocks of 128 rows) no expert is named more than 32 times, and in every such block some expert is named exactly 32 times.
All inputs are finite; a program needn't handle non-finite values.
Results may differ from a plain program's by a relative error of at most 0.0095.
Values may be sent and summed in bfloat16 or wider, within the bound.
A program may use at most 64 MiB of HBM per device.

v0:
```python
import jax
import jax.numpy as jnp
from jax import lax
from jax.experimental import pallas as pl
from jax.experimental.pallas import tpu as pltpu
from jax.sharding import PartitionSpec as P

EPSILON = 1e-06
GROUPS = 4
SPLIT = 2
LANES = 128
SUBLANES = 8
MESH = pl.DeviceIdType.MESH
COLUMNS, LATE = (2, 5, 1, 0, 3, 4, 6, 7), 4
OUTER, OUTER_PARTS = (6, 3, 4, 2, 5, 7), 1
INNER, INNER_PARTS = (3, 6, 4, 7, 2, 5), 2
PLAN = (
    "f1 z6 x0 z3",
    "m0 c0 x6 z4",
    "c6 z2 h6 b6",
    "x1 x4 c4 x3",
    "z7 c3 e6 z5",
    "h4 x2 c1 x7",
    "b4 c7 h3 h0",
    "h1 b3 x5 h7",
    "b7 e4 c2 c5",
    "h2 h5 b5 b2",
    "b1 b0 e3 e7",
    "e5 e2 e1 e0",
)


def flipped(index, mask, size):
    total, bit = 0, 1
    while bit < size:
        total = total + ((index // bit + mask // bit) % 2) * bit
        bit *= 2
    return total


def gray(index):
    return flipped(index, index // 2, 4)


def layer_kernel(
    value_hbm, gate_hbm_in, kernel_hbm, bias_hbm, lgain_hbm, lbias_hbm, ogain_hbm, res_hbm, mgain_hbm, ids_hbm, shares_hbm,
    out_hbm, gate_hbm, up_hbm, down_hbm, result,
    value, gate, kernel, params, residual, moe_gain, ids, shares,
    w_out, w_gate, w_up, w_down, taps, meta, pick, unpick, padded, halo_out, halo_in, conv, wide, gains, branch, hid,
    send, back, rows, normed, weights, own, half_out, half_in, cross_out, cross_in, final, act, total,
    load_sem, in_sem, meta_s, meta_r, halo_s, halo_r, gain_s, gain_r, group_s, group_r,
    z_s, z_r, pair_s, pair_r, x_s, x_r, via_s, via_r,
    half_s, half_r, cross_s, cross_r, back_s, back_r,
):
    spn, tpn = weights.shape[:2]
    pieces, _, height, width = rows.shape
    cap = height * SPLIT
    last = pieces - 1
    me_z, me_t = lax.axis_index("sp"), lax.axis_index("tp")
    pair, across = flipped(me_t, 1, tpn), flipped(me_t, 2, tpn)
    hidden = w_gate.shape[1]
    tok_rows, channels = value.shape
    row_count = tok_rows // tpn
    full = channels * tpn
    reach = padded.shape[0] - tok_rows
    tap_count = kernel.shape[0]
    f32, bf = jnp.float32, jnp.bfloat16

    def to(z, t):
        return {"sp": z, "tp": t}

    def copy(src, dst, s, r, z, t):
        return pltpu.make_async_remote_copy(
            src_ref=src, dst_ref=dst, send_sem=s, recv_sem=r, device_id=to(z, t), device_id_type=MESH
        )

    peers = [(q, r) for q in range(spn) for r in range(tpn) if q or r]
    barrier = pltpu.get_barrier_semaphore()
    for q, r in peers:
        pl.semaphore_signal(
            barrier, inc=1, device_id=to(flipped(me_z, gray(q), spn), flipped(me_t, r, tpn)), device_id_type=MESH
        )

    inputs = [
        pltpu.make_async_copy(a, b, in_sem.at[i])
        for i, (a, b) in enumerate((
            (value_hbm, value), (gate_hbm_in, gate), (kernel_hbm, kernel), (bias_hbm, params.at[pl.ds(3, 1)]),
            (lgain_hbm, params.at[pl.ds(0, 1)]), (lbias_hbm, params.at[pl.ds(1, 1)]),
            (ogain_hbm, params.at[pl.ds(2, 1)]), (ids_hbm, ids), (shares_hbm, shares),
            (res_hbm, residual), (mgain_hbm, moe_gain),
        ))
    ]
    loads = [
        pltpu.make_async_copy(a, b, load_sem.at[i])
        for i, (a, b) in enumerate(((out_hbm, w_out), (gate_hbm, w_gate), (up_hbm, w_up), (down_hbm, w_down)))
    ]
    for load in inputs + loads:
        load.start()

    for load in inputs[:7]:
        load.wait()
    taps[:tap_count, :] = kernel[...].astype(f32)
    gated = (value[...].astype(f32) / (1.0 + jnp.exp(-gate[...].astype(f32)))).astype(bf)
    padded[reach:, :] = gated.astype(f32)
    halo_out[...] = gated[tok_rows - reach :]

    mine = pl.ds(pl.multiple_of(me_t * channels, channels), channels)

    def halo_copy(z):
        return copy(halo_out, halo_in, halo_s.at[0], halo_r.at[0], z, me_t)

    def gain_copy(r):
        return copy(params, gains.at[:, mine], gain_s.at[r], gain_r.at[r], me_z, flipped(me_t, r, tpn))

    def group_copy(t, low, high):
        span = pl.ds(low, high - low)
        r = flipped(me_t, t, tpn)
        return copy(conv.at[t, span], wide.at[span, mine], group_s.at[r], group_r.at[r], me_z, t)

    def z_copy(k, cols=pl.ds(0, width)):
        return copy(
            send.at[k, :, cols], rows.at[k, 0, :, cols], z_s.at[k], z_r.at[k],
            flipped(me_z, gray(k // SPLIT), spn), me_t,
        )

    def meta_copy(q, r):
        return copy(
            meta.at[q], weights.at[q, r], meta_s.at[q, r], meta_r.at[q, r],
            flipped(me_z, gray(q), spn), flipped(me_t, r, tpn),
        )

    def pair_copy(k):
        return copy(rows.at[k, 0], rows.at[k, 1], pair_s.at[k], pair_r.at[k], me_z, pair)

    def x_copy(k, cols=pl.ds(0, width)):
        return copy(
            rows.at[k, 0, :, cols], rows.at[k, 2, :, cols], x_s.at[k], x_r.at[k], me_z, across
        )

    def via_copy(k):
        return copy(rows.at[k, 2], rows.at[k, 3], via_s.at[k], via_r.at[k], me_z, pair)

    def half_copy(k):
        return copy(half_out.at[k], half_in.at[k], half_s.at[k], half_r.at[k], me_z, pair)

    def cross_copy(k):
        return copy(cross_out.at[k], cross_in.at[k], cross_s.at[k], cross_r.at[k], me_z, across)

    def back_copy(k):
        return copy(
            final.at[k], back.at[COLUMNS.index(k)], back_s.at[k], back_r.at[k], flipped(me_z, gray(k // SPLIT), spn), me_t
        )

    def convolve(block, first, count):
        start = pl.multiple_of(block * row_count + first, SUBLANES)
        for c in range(0, channels, LANES):
            window = padded[pl.ds(start, count + reach), c : c + LANES]
            sums = jnp.zeros((count, LANES), f32) + params[3:4, c : c + LANES]
            for b in range(SUBLANES):
                extent = count + (SUBLANES if b else 0)
                group = None
                for a in range(0, reach + 1, SUBLANES):
                    tap = a + b - (reach - tap_count + 1)
                    if 0 <= tap < tap_count:
                        term = window[a : a + extent] * taps[tap : tap + 1, c : c + LANES]
                        group = term if group is None else group + term
                sums = sums + group[b : b + count]
            conv[block, first : first + count, c : c + LANES] = sums.astype(bf)

    side = me_t // 2
    for j, b in enumerate((2, 3, 1, 0)):
        block = b + side * (3 - 2 * b)
        edge = b in (0, 3)
        convolve(block, reach, row_count - reach)
        if edge:
            @pl.when(block != 0)
            def _():
                convolve(block, 0, reach)
        else:
            convolve(block, 0, reach)
        if j == 0:
            pl.semaphore_wait(barrier, len(peers))

            @pl.when(me_z < spn - 1)
            def _():
                halo_copy(me_z + 1).start()

            for r in range(1, tpn):
                gain_copy(r).start()

        if edge:
            @pl.when((block != me_t) & (block != 0))
            def _():
                group_copy(block, 0, row_count).start()

            @pl.when((block != me_t) & (block == 0))
            def _():
                group_copy(block, reach, row_count).start()
        else:
            @pl.when(block != me_t)
            def _():
                group_copy(block, 0, row_count).start()

    @pl.when(me_z == 0)
    def _():
        padded[:reach, :] = jnp.zeros((reach, channels), f32)

    @pl.when(me_z > 0)
    def _():
        halo_copy(me_z - 1).wait_recv()
        padded[:reach, :] = halo_in[...].astype(f32)

    convolve(0, 0, reach)

    @pl.when(me_t != 0)
    def _():
        group_copy(0, 0, reach).start()

    wide[:, mine] = conv[me_t]
    gains[:, mine] = params[...]

    for load in inputs[7:9]:
        load.wait()
    square = (row_count, row_count)
    down, along = (lax.broadcasted_iota(jnp.int32, square, d) for d in (0, 1))

    def upright(line):
        return jnp.sum(
            jnp.where(down == along, jnp.broadcast_to(line, square), jnp.zeros((), line.dtype)),
            axis=1, keepdims=True,
        )

    def distance(number):
        mask = jnp.bitwise_xor(number, me_z)
        return jnp.bitwise_xor(mask, lax.div(mask, 2))

    def place(number, order):
        found = distance(number) * SPLIT + lax.div(order, height)
        column = sum(jnp.where(found == k, c, 0) for c, k in enumerate(COLUMNS))
        return column * height + lax.rem(order, height)

    group_row = jnp.broadcast_to(lax.div(ids[0:1, :], tpn), square)
    group = jnp.broadcast_to(upright(group_row[0:1, :]), square)
    same = group == group_row
    rank = jnp.sum(jnp.where(same & (along < down), 1, 0), axis=1, keepdims=True)
    rank_row = jnp.sum(jnp.where(same & (down < along), 1, 0), axis=0, keepdims=True)
    slot = place(group[:, 0:1], rank)
    slot_row = place(group_row[0:1, :], rank_row)
    slots = spn * cap
    pick[...] = jnp.where(
        lax.broadcasted_iota(jnp.int32, (slots, row_count), 0) == slot_row, 1.0, 0.0
    ).astype(bf)
    unpick[...] = jnp.where(
        lax.broadcasted_iota(jnp.int32, (row_count, slots), 1) == slot, 1.0, 0.0
    ).astype(bf)
    lane = lax.broadcasted_iota(jnp.int32, (row_count, LANES), 1)
    experts = lax.rem(ids[...], tpn)
    meta[...] = jnp.zeros_like(meta)
    by_expert = [
        upright(jnp.sum(jnp.where(experts == e, shares[...], 0.0), axis=0, keepdims=True))
        for e in range(tpn)
    ]
    for q in range(spn):
        here = (distance(group[:, 0:1]) == q) & (lane == rank)
        for e in range(tpn):
            share = by_expert[e]
            meta[q, e : e + 1, :] = jnp.sum(jnp.where(here, share, 0.0), axis=0, keepdims=True)
    weights[0, 0] = meta[0]
    for q, r in peers:
        meta_copy(q, r).start()

    for load in inputs[9:]:
        load.wait()
    loads[0].wait()
    for r in range(1, tpn):
        gain_copy(r).wait_recv()
    for r in range(1, tpn):
        t = flipped(me_t, r, tpn)
        group_copy(t, 0, row_count).wait_recv()

    part = min(row_count, 32)
    for first in range(0, row_count, part):
        v = wide[first : first + part, :].astype(f32)
        average = jnp.sum(v, axis=1, keepdims=True) / full
        spread = jnp.sum(v * v, axis=1, keepdims=True) / full - average * average
        v = (v - average) * lax.rsqrt(spread + EPSILON) * gains[0:1, :] + gains[1:2, :]
        v = v / (1.0 + jnp.exp(-v))
        energy = jnp.sum(v * v, axis=1, keepdims=True) / full
        branch[first : first + part, :] = (v * lax.rsqrt(energy + EPSILON) * gains[2:3, :]).astype(bf)

    tile = min(hidden, 512)
    inner = (me_z > 0) & (me_z < spn - 1)

    def project(c, carry):
        cols = pl.ds(pl.multiple_of(c * tile, tile), tile)
        h = residual[:, cols].astype(f32) + jnp.dot(
            branch[...], w_out[:, cols], preferred_element_type=f32
        )
        h = h.astype(bf)
        hid[:, cols] = h
        picked = jnp.dot(pick[...], h, preferred_element_type=f32).astype(bf)
        for k in range(pieces):
            at = COLUMNS.index(k) * height
            taken = picked[at : at + height]
            if k < SPLIT:
                rows[k, 0, :, cols] = taken
            else:
                send[k, :, cols] = taken
        x_copy(0, cols).start()

        @pl.when(inner)
        def _():
            for k in INNER[:INNER_PARTS]:
                z_copy(k, cols).start()

        @pl.when(jnp.logical_not(inner))
        def _():
            for k in OUTER[:OUTER_PARTS]:
                z_copy(k, cols).start()

        return carry

    lax.fori_loop(0, width // tile, project, 0)
    pair_copy(0).start()

    @pl.when(inner)
    def _():
        for k in INNER[INNER_PARTS:]:
            z_copy(k).start()

    @pl.when(jnp.logical_not(inner))
    def _():
        for k in OUTER[OUTER_PARTS:]:
            z_copy(k).start()


    row_of, lane_of = (lax.broadcasted_iota(jnp.int32, (height, LANES), d) for d in (0, 1))

    def compute(k):
        strip = height // 2
        for r in range(tpn):
            for first in range(0, height, strip):
                h = rows[k, r, first : first + strip].astype(f32)
                level = lax.rsqrt(jnp.sum(h * h, axis=1, keepdims=True) / width + EPSILON)
                low = r * height + first
                normed[low : low + strip] = (h * level * moe_gain[...]).astype(bf)
        x = normed[...]
        diagonal = lane_of == row_of + (k % SPLIT) * height
        for c in range(0, hidden, 256):
            g = jnp.dot(x, w_gate[:, c : c + 256], preferred_element_type=jnp.float32)
            u = jnp.dot(x, w_up[:, c : c + 256], preferred_element_type=jnp.float32)
            act[:, c : c + 256] = (g / (1.0 + jnp.exp(-g)) * u).astype(jnp.bfloat16)
        a = act[...]
        scales = [
            jnp.sum(jnp.where(diagonal, weights[k // SPLIT, r, pl.ds(me_t, 1), :], 0.0), axis=1, keepdims=True)
            for r in range(tpn)
        ]

        def column(c, carry):
            cols = pl.ds(pl.multiple_of(c * tile, tile), tile)
            res = jnp.dot(a, w_down[:, cols], preferred_element_type=jnp.float32).astype(jnp.bfloat16)
            res = res.astype(jnp.float32)
            parts = [res[r * height : (r + 1) * height] * scales[r] for r in range(tpn)]
            half_out[k, 0, :, cols] = parts[1].astype(jnp.bfloat16)
            half_out[k, 1, :, cols] = parts[3].astype(jnp.bfloat16)
            own[k, 0, :, cols] = parts[0]
            own[k, 1, :, cols] = parts[2]
            return carry

        lax.fori_loop(0, width // tile, column, 0)

    def first(k):
        x_copy(k).start()
        pair_copy(k).start()

    def forward(k):
        z_copy(k).wait_recv()
        first(k)

    def relay(k):
        x_copy(k).wait_recv()
        via_copy(k).start()

    def run(k):
        pair_copy(k).wait_recv()
        via_copy(k).wait_recv()
        compute(k)
        half_copy(k).start()

    def halve(k):
        half_copy(k).wait_recv()
        cross_out[k] = (own[k, 1] + half_in[k, 1].astype(jnp.float32)).astype(jnp.bfloat16)

    def cross(k):
        cross_copy(k).start()

    def finish(k):
        cross_copy(k).wait_recv()
        ready = (
            own[k, 0] + half_in[k, 0].astype(jnp.float32) + cross_in[k].astype(jnp.float32)
        ).astype(jnp.bfloat16)
        if k < SPLIT:
            back[COLUMNS.index(k)] = ready
        else:
            final[k] = ready
            back_copy(k).start()

    def arrive(k):
        for q, r in peers:
            meta_copy(q, r).wait_recv()
        for load in loads[1:]:
            load.wait()

    acts = {"m": arrive, "f": first, "z": forward, "x": relay, "c": run, "h": halve, "b": cross, "e": finish}
    for line in PLAN:
        for word in line.split():
            acts[word[0]](int(word[1:]))

    edge = LATE * height
    for k in COLUMNS[LATE:]:
        if k >= SPLIT:
            back_copy(k).wait_recv()
    for c in range(0, width, tile):
        moved = back[LATE:, :, c : c + tile].reshape((pieces - LATE) * height, tile)
        total[:, c : c + tile] = hid[:, c : c + tile].astype(f32) + jnp.dot(
            unpick[:, edge:], moved, preferred_element_type=f32
        )
    for k in COLUMNS[:LATE]:
        if k >= SPLIT:
            back_copy(k).wait_recv()

    for c in range(0, width, tile):
        moved = back[:LATE, :, c : c + tile].reshape(edge, tile)
        result[:, c : c + tile] = (
            total[:, c : c + tile] + jnp.dot(unpick[:, :edge], moved, preferred_element_type=f32)
        ).astype(bf)

    @pl.when(me_z < spn - 1)
    def _():
        halo_copy(me_z + 1).wait_send()

    for r in range(1, tpn):
        gain_copy(r).wait_send()
        group_copy(flipped(me_t, r, tpn), 0, row_count).wait_send()
    for q, r in peers:
        meta_copy(q, r).wait_send()
    for k in range(pieces):
        for make in (x_copy, pair_copy, via_copy, half_copy, cross_copy):
            make(k).wait_send()
    for k in range(SPLIT, pieces):
        z_copy(k).wait_send()
        back_copy(k).wait_send()


def fused_layer(
    conv_value,
    conv_gate,
    kernel,
    conv_bias,
    ln_gain,
    ln_bias,
    out_gain,
    out_weight,
    residual,
    moe_gain,
    expert_ids,
    expert_weights,
    w_gate,
    w_up,
    w_down,
):
    spn, tpn = lax.axis_size("sp"), lax.axis_size("tp")
    tok_rows, channels = conv_value.shape
    row_count, width = residual.shape
    hidden = w_gate.shape[2]
    capacity = 2 * row_count // min(row_count, spn * tpn // 2)
    cap = tpn * capacity // 2
    pieces, height = spn * SPLIT, cap // SPLIT
    reach = -(-(kernel.shape[0] - 1) // SUBLANES) * SUBLANES
    bf, f32, dma = jnp.bfloat16, jnp.float32, pltpu.SemaphoreType.DMA
    hbm = pl.BlockSpec(memory_space=pl.ANY)
    return pl.pallas_call(
        layer_kernel,
        out_shape=pltpu.VMEM((row_count, width), bf),
        in_specs=[hbm] * 15,
        out_specs=pl.BlockSpec(memory_space=pltpu.VMEM),
        scratch_shapes=[
            pltpu.VMEM(conv_value.shape, bf),
            pltpu.VMEM(conv_gate.shape, bf),
            pltpu.VMEM(kernel.shape, bf),
            pltpu.VMEM((4, channels), f32),
            pltpu.VMEM(residual.shape, bf),
            pltpu.VMEM((1, width), f32),
            pltpu.VMEM((2, row_count), jnp.int32),
            pltpu.VMEM((2, row_count), f32),
            pltpu.VMEM(out_weight.shape, bf),
            pltpu.VMEM(w_gate.shape[1:], bf),
            pltpu.VMEM(w_up.shape[1:], bf),
            pltpu.VMEM(w_down.shape[1:], bf),
            pltpu.VMEM((reach + SUBLANES, channels), f32),
            pltpu.VMEM((spn, SUBLANES, LANES), f32),
            pltpu.VMEM((spn * cap, row_count), bf),
            pltpu.VMEM((row_count, spn * cap), bf),
            pltpu.VMEM((reach + tok_rows, channels), f32),
            pltpu.VMEM((reach, channels), bf),
            pltpu.VMEM((reach, channels), bf),
            pltpu.VMEM((tpn, row_count, channels), bf),
            pltpu.VMEM((row_count, channels * tpn), bf),
            pltpu.VMEM((4, channels * tpn), f32),
            pltpu.VMEM((row_count, channels * tpn), bf),
            pltpu.VMEM((row_count, width), bf),
            pltpu.VMEM((pieces, height, width), bf),
            pltpu.VMEM((pieces, height, width), bf),
            pltpu.VMEM((pieces, tpn, height, width), bf),
            pltpu.VMEM((tpn * height, width), bf),
            pltpu.VMEM((spn, tpn, SUBLANES, LANES), f32),
            pltpu.VMEM((pieces, 2, height, width), f32),
            pltpu.VMEM((pieces, 2, height, width), bf),
            pltpu.VMEM((pieces, 2, height, width), bf),
            pltpu.VMEM((pieces, height, width), bf),
            pltpu.VMEM((pieces, height, width), bf),
            pltpu.VMEM((pieces, height, width), bf),
            pltpu.VMEM((tpn * height, hidden), bf),
            pltpu.VMEM((row_count, width), f32),
            dma((4,)),
            dma((11,)),
            dma((spn, tpn)),
            dma((spn, tpn)),
            dma((1,)),
            dma((1,)),
        ]
        + [dma((tpn,))] * 4
        + [dma((pieces,))] * 14,
        compiler_params=pltpu.CompilerParams(collective_id=0, has_side_effects=True),
    )(
        conv_value, conv_gate, kernel, conv_bias[None, :], ln_gain[None, :], ln_bias[None, :],
        out_gain[None, :], residual, moe_gain[None, :], expert_ids.T, expert_weights.T,
        out_weight, w_gate[0], w_up[0], w_down[0],
    )


def passed_along(block, axis, distance):
    devices = range(lax.axis_size(axis))
    route = [(i - distance, i) for i in devices if i - distance in devices]
    return lax.ppermute(block, axis, route)


def per_device(
    conv_value,
    conv_gate,
    kernel,
    conv_bias,
    ln_gain,
    ln_bias,
    out_gain,
    out_weight,
    residual,
    moe_gain,
    expert_ids,
    expert_weights,
    w_gate,
    w_up,
    w_down,
):
    tpn = lax.axis_size("tp")
    if lax.axis_size("sp") == GROUPS and tpn == 4:
        return fused_layer(
            conv_value, conv_gate, kernel, conv_bias, ln_gain, ln_bias, out_gain, out_weight, residual,
            moe_gain, expert_ids, expert_weights, w_gate, w_up, w_down,
        )
    tok_rows, channels = conv_value.shape
    reach_rows = kernel.shape[0] - 1
    full_channels = channels * lax.axis_size("tp")
    gated = (conv_value.astype(jnp.float32) * jax.nn.sigmoid(conv_gate.astype(jnp.float32))).astype(
        jnp.bfloat16
    )
    before = passed_along(gated[tok_rows - reach_rows :], "sp", 1)
    padded = jnp.concatenate([before, gated], axis=0)
    convolved = jnp.zeros((tok_rows, channels), jnp.float32) + conv_bias
    for offset in range(reach_rows + 1):
        convolved = convolved + padded[offset : offset + tok_rows].astype(jnp.float32) * kernel[
            offset
        ].astype(jnp.float32)
    totals = lax.psum((jnp.sum(convolved, axis=1), jnp.sum(convolved * convolved, axis=1)), "tp")
    average = (totals[0] / full_channels)[:, None]
    spread = (totals[1] / full_channels)[:, None] - average * average
    swished = jax.nn.silu((convolved - average) * lax.rsqrt(spread + EPSILON) * ln_gain + ln_bias)
    energy = lax.psum(jnp.sum(swished * swished, axis=1), "tp")
    branch = (swished * lax.rsqrt(energy / full_channels + EPSILON)[:, None] * out_gain).astype(
        jnp.bfloat16
    )
    row_count = tok_rows // lax.axis_size("tp")
    regrouped = lax.all_to_all(branch, "tp", split_axis=0, concat_axis=1, tiled=True)
    projected = jnp.dot(regrouped, out_weight, preferred_element_type=jnp.float32)
    hidden = (residual.astype(jnp.float32) + projected).astype(jnp.bfloat16)
    widened = hidden.astype(jnp.float32)
    normed = (
        widened * lax.rsqrt(jnp.mean(widened * widened, axis=1, keepdims=True) + EPSILON) * moe_gain
    ).astype(jnp.bfloat16)
    width = normed.shape[1]
    experts = lax.axis_size("sp") * lax.axis_size("tp")
    capacity = 2 * row_count // min(row_count, experts // 2)
    flat_ids = expert_ids.reshape(-1)
    onehot = (flat_ids[:, None] == jnp.arange(experts, dtype=jnp.int32)[None, :]).astype(jnp.int32)
    slot_rank = jnp.sum((jnp.cumsum(onehot, axis=0) - 1) * onehot, axis=1)
    position = flat_ids * capacity + slot_rank
    outgoing = (
        jnp.zeros((experts * capacity, width), jnp.bfloat16)
        .at[position]
        .set(jnp.repeat(normed, 2, axis=0))
    )
    outgoing = outgoing.reshape(experts, capacity, width)
    arriving = lax.all_to_all(outgoing, ("sp", "tp"), split_axis=0, concat_axis=0, tiled=True)
    flattened = arriving.reshape(-1, width)
    gate_part = jnp.dot(flattened, w_gate[0], preferred_element_type=jnp.float32)
    up_part = jnp.dot(flattened, w_up[0], preferred_element_type=jnp.float32)
    active = (jax.nn.silu(gate_part) * up_part).astype(jnp.bfloat16)
    result = jnp.dot(active, w_down[0], preferred_element_type=jnp.float32).astype(jnp.bfloat16)
    produced = result.reshape(arriving.shape)
    returned = lax.all_to_all(produced, ("sp", "tp"), split_axis=0, concat_axis=0, tiled=True)
    returned = returned.reshape(experts * capacity, width)
    picked = returned[position].reshape(row_count, 2, width)
    combined = jnp.sum(picked.astype(jnp.float32) * expert_weights[:, :, None], axis=1)
    return (widened + combined).astype(jnp.bfloat16)


def solution(mesh):
    in_specs = (
        P(("grp", "sp"), "tp"),
        P(("grp", "sp"), "tp"),
        P(None, "tp"),
        P("tp"),
        P("tp"),
        P("tp"),
        P("tp"),
        P(),
        P(("grp", "sp", "tp"), None),
        P(),
        P(("grp", "sp", "tp"), None),
        P(("grp", "sp", "tp"), None),
        P(("sp", "tp"), None, None),
        P(("sp", "tp"), None, None),
        P(("sp", "tp"), None, None),
    )
    out_specs = P(("grp", "sp", "tp"), None)
    return jax.shard_map(
        per_device, mesh=mesh, in_specs=in_specs, out_specs=out_specs, check_vma=False
    )
```

profile of v0, /device:TPU:0, one launch (start us, length us, event | category | flops | bytes accessed | tf_op | source)
XLA Modules:
  0.0 65.6 jit_solution(15567815855370376235)
XLA Ops:
  0.0 64.8 %shard_map.145 = bf16[128,2048]{1,0:T(8,128)(2,1)S(1)} custom-call(bf16[512,256]{1,0:T(8,128)(2,1)} %value_hbm.1, bf16[512,256]{1,0:T(8,128)(2,1)} %gate_hbm_in.1, bf16[31,256]{1,0:T(8,128)(2,1)} %kernel_hbm.1, f32[1,256]{1,0:T(1,128)} %bitcast.14, f32[1,256]{1,0:T(1,128)} %bitcast.15, f32[1,256]{1,0:T(1,128)} %bitcast.16, f32[1,256]{1,0:T(1,128)} %bitcast.17, ...), custom_call_target="tpu_custom_call" | custom-call | tf_op jit(solution)/shard_map/pallas_call | solution.py:482
  64.8 0.8 %copy.17 = bf16[128,2048]{1,0:T(8,128)(2,1)} copy(bf16[128,2048]{1,0:T(8,128)(2,1)S(1)} %shard_map.145) | data formatting | bytes 1048576
where the time goes:
time: 65.8 us; the launch traced here: 65.6 us
  Pallas kernels  64.8 us (98%)
  local copies, waits for them, and re-layouts  0.8 us (1%)
    pallas_call x1, Pallas kernels, fused_layer(): pl.pallas_call(layer_kernel, out_shape=pltpu.VMEM((row_count, width), bf)...  64.8 us

commit v1 on v0

--- a/solution.py
+++ b/solution.py
@@ -48,7 +48,7 @@
     value, gate, kernel, params, residual, moe_gain, ids, shares,
     w_out, w_gate, w_up, w_down, taps, meta, pick, unpick, padded, halo_out, halo_in, conv, wide, gains, branch, hid,
     send, back, rows, normed, weights, own, half_out, half_in, cross_out, cross_in, final, act, total,
-    load_sem, in_sem, meta_s, meta_r, halo_s, halo_r, gain_s, gain_r, group_s, group_r,
+    low, high, load_sem, in_sem, meta_s, meta_r, halo_s, halo_r, gain_s, gain_r, group_s, group_r,
     z_s, z_r, pair_s, pair_r, x_s, x_r, via_s, via_r,
     half_s, half_r, cross_s, cross_r, back_s, back_r,
 ):
@@ -75,11 +75,39 @@
         )
 
     peers = [(q, r) for q in range(spn) for r in range(tpn) if q or r]
+    below, above = me_z > 0, me_z < spn - 1
     barrier = pltpu.get_barrier_semaphore()
-    for q, r in peers:
-        pl.semaphore_signal(
-            barrier, inc=1, device_id=to(flipped(me_z, gray(q), spn), flipped(me_t, r, tpn)), device_id_type=MESH
-        )
+
+    def tell(semaphore, z, t):
+        pl.semaphore_signal(semaphore, inc=1, device_id=to(z, t), device_id_type=MESH)
+
+    for r in range(1, tpn):
+        tell(barrier, me_z, flipped(me_t, r, tpn))
+
+    @pl.when(below)
+    def _():
+        tell(barrier, me_z - 1, me_t)
+
+    @pl.when(above)
+    def _():
+        tell(barrier, me_z + 1, me_t)
+
+    def pass_on(d):
+        @pl.when(me_z >= d)
+        def _():
+            pl.semaphore_wait(low.at[d], 1)
+
+            @pl.when(above)
+            def _():
+                tell(low.at[d + 1], me_z + 1, me_t)
+
+        @pl.when(me_z + d < spn)
+        def _():
+            pl.semaphore_wait(high.at[d], 1)
+
+            @pl.when(below)
+            def _():
+                tell(high.at[d + 1], me_z - 1, me_t)
 
     inputs = [
         pltpu.make_async_copy(a, b, in_sem.at[i])
@@ -179,11 +207,16 @@
         else:
             convolve(block, 0, reach)
         if j == 0:
-            pl.semaphore_wait(barrier, len(peers))
-
-            @pl.when(me_z < spn - 1)
+            pl.semaphore_wait(barrier, tpn - 1 + jnp.where(below & above, 2, 1))
+
+            @pl.when(above)
             def _():
                 halo_copy(me_z + 1).start()
+                tell(low.at[1], me_z + 1, me_t)
+
+            @pl.when(below)
+            def _():
+                tell(high.at[1], me_z - 1, me_t)
 
             for r in range(1, tpn):
                 gain_copy(r).start()
@@ -219,6 +252,7 @@
     wide[:, mine] = conv[me_t]
     gains[:, mine] = params[...]
 
+    pass_on(1)
     for load in inputs[7:9]:
         load.wait()
     square = (row_count, row_count)
@@ -266,6 +300,8 @@
             share = by_expert[e]
             meta[q, e : e + 1, :] = jnp.sum(jnp.where(here, share, 0.0), axis=0, keepdims=True)
     weights[0, 0] = meta[0]
+    for d in range(2, spn):
+        pass_on(d)
     for q, r in peers:
         meta_copy(q, r).start()
 
@@ -522,6 +558,8 @@
             pltpu.VMEM((pieces, height, width), bf),
             pltpu.VMEM((tpn * height, hidden), bf),
             pltpu.VMEM((row_count, width), f32),
+            pltpu.SemaphoreType.REGULAR((spn + 1,)),
+            pltpu.SemaphoreType.REGULAR((spn + 1,)),
             dma((4,)),
             dma((11,)),
             dma((spn, tpn)),

time: 65.8 us -> 64.7 us (0.983)
  Pallas kernels: 64.8 us -> 63.7 us
    pallas_call x1, Pallas kernels: 64.8 us -> 63.7 us  [fused_layer(): pl.pallas_call(layer_kernel, out_shape=pltpu.VMEM((row_count, width), bf)...]
where the time goes in v1:
time: 64.7 us; the launch traced here: 64.5 us
  Pallas kernels  63.7 us (98%)
  local copies, waits for them, and re-layouts  0.8 us (1%)
    pallas_call x1, Pallas kernels, fused_layer(): pl.pallas_call(layer_kernel, out_shape=pltpu.VMEM((row_count, width), bf)...  63.7 us

profile of v1, /device:TPU:0, one launch (start us, length us, event | category | flops | bytes accessed | tf_op | source)
XLA Modules:
  0.0 64.5 jit_solution(11043019289161658331)
XLA Ops:
  0.0 63.7 %shard_map.145 = bf16[128,2048]{1,0:T(8,128)(2,1)S(1)} custom-call(bf16[512,256]{1,0:T(8,128)(2,1)} %value_hbm.1, bf16[512,256]{1,0:T(8,128)(2,1)} %gate_hbm_in.1, bf16[31,256]{1,0:T(8,128)(2,1)} %kernel_hbm.1, f32[1,256]{1,0:T(1,128)} %bitcast.14, f32[1,256]{1,0:T(1,128)} %bitcast.15, f32[1,256]{1,0:T(1,128)} %bitcast.16, f32[1,256]{1,0:T(1,128)} %bitcast.17, ...), custom_call_target="tpu_custom_call" | custom-call | tf_op jit(solution)/shard_map/pallas_call | solution.py:518
  63.8 0.8 %copy.17 = bf16[128,2048]{1,0:T(8,128)(2,1)} copy(bf16[128,2048]{1,0:T(8,128)(2,1)S(1)} %shard_map.145) | data formatting | bytes 1048576

commit v2 on v1

--- a/solution.py
+++ b/solution.py
@@ -11,22 +11,22 @@
 LANES = 128
 SUBLANES = 8
 MESH = pl.DeviceIdType.MESH
-COLUMNS, LATE = (2, 5, 1, 0, 3, 4, 6, 7), 4
-OUTER, OUTER_PARTS = (6, 3, 4, 2, 5, 7), 1
-INNER, INNER_PARTS = (3, 6, 4, 7, 2, 5), 2
+COLUMNS, LATE = (2, 7, 1, 0, 3, 4, 5, 6), 4
+OUTER, OUTER_PARTS = (4, 3, 2, 5, 7, 6), 1
+INNER, INNER_PARTS = (4, 5, 3, 6, 7, 2), 1
 PLAN = (
-    "f1 z6 x0 z3",
-    "m0 c0 x6 z4",
-    "c6 z2 h6 b6",
-    "x1 x4 c4 x3",
-    "z7 c3 e6 z5",
-    "h4 x2 c1 x7",
-    "b4 c7 h3 h0",
-    "h1 b3 x5 h7",
-    "b7 e4 c2 c5",
-    "h2 h5 b5 b2",
-    "b1 b0 e3 e7",
-    "e5 e2 e1 e0",
+    "f1 x0 z4 z3",
+    "m0 c0 x1 x4",
+    "z2 c4 z5 c1",
+    "x3 h4 x2 h1",
+    "b4 c3 z6 x5",
+    "c5 z7 h3 h5",
+    "b5 x6 b3 h0",
+    "e4 c2 c6 x7",
+    "h2 h6 b6 e5",
+    "c7 e3 b2 h7",
+    "b7 e6 b1 b0",
+    "e2 e7 e1 e0",
 )
 
 
@@ -356,7 +356,8 @@
 
         return carry
 
-    lax.fori_loop(0, width // tile, project, 0)
+    for c in range(width // tile):
+        project(c, 0)
     pair_copy(0).start()
 
     @pl.when(inner)

time: 64.7 us -> 64.3 us (level)
  no operation moved by 1% of the time
where the time goes in v2:
time: 64.3 us; the launch traced here: 64.1 us
  Pallas kernels  63.3 us (98%)
  local copies, waits for them, and re-layouts  0.8 us (1%)
    pallas_call x1, Pallas kernels, fused_layer(): pl.pallas_call(layer_kernel, out_shape=pltpu.VMEM((row_count, width), bf)...  63.3 us

profile of v2, /device:TPU:0, one launch (start us, length us, event | category | flops | bytes accessed | tf_op | source)
XLA Modules:
  0.0 64.1 jit_solution(9356143706449662054)
XLA Ops:
  0.0 63.3 %shard_map.145 = bf16[128,2048]{1,0:T(8,128)(2,1)S(1)} custom-call(bf16[512,256]{1,0:T(8,128)(2,1)} %value_hbm.1, bf16[512,256]{1,0:T(8,128)(2,1)} %gate_hbm_in.1, bf16[31,256]{1,0:T(8,128)(2,1)} %kernel_hbm.1, f32[1,256]{1,0:T(1,128)} %bitcast.14, f32[1,256]{1,0:T(1,128)} %bitcast.15, f32[1,256]{1,0:T(1,128)} %bitcast.16, f32[1,256]{1,0:T(1,128)} %bitcast.17, ...), custom_call_target="tpu_custom_call" | custom-call | tf_op jit(solution)/shard_map/pallas_call | solution.py:519
  63.3 0.8 %copy.17 = bf16[128,2048]{1,0:T(8,128)(2,1)} copy(bf16[128,2048]{1,0:T(8,128)(2,1)S(1)} %shard_map.145) | data formatting | bytes 1048576

commit v3 on v2

--- a/solution.py
+++ b/solution.py
@@ -122,11 +122,13 @@
         pltpu.make_async_copy(a, b, load_sem.at[i])
         for i, (a, b) in enumerate(((out_hbm, w_out), (gate_hbm, w_gate), (up_hbm, w_up), (down_hbm, w_down)))
     ]
-    for load in inputs + loads:
+    for load in inputs:
         load.start()
 
     for load in inputs[:7]:
         load.wait()
+    for load in loads:
+        load.start()
     taps[:tap_count, :] = kernel[...].astype(f32)
     gated = (value[...].astype(f32) / (1.0 + jnp.exp(-gate[...].astype(f32)))).astype(bf)
     padded[reach:, :] = gated.astype(f32)

time: 64.3 us -> 64.3 us (level)
  no operation moved by 1% of the time
where the time goes in v3:
time: 64.3 us; the launch traced here: 64.1 us
  Pallas kernels  63.3 us (98%)
  local copies, waits for them, and re-layouts  0.8 us (1%)
    pallas_call x1, Pallas kernels, fused_layer(): pl.pallas_call(layer_kernel, out_shape=pltpu.VMEM((row_count, width), bf)...  63.3 us

profile of v3, /device:TPU:0, one launch (start us, length us, event | category | flops | bytes accessed | tf_op | source)
XLA Modules:
  0.0 64.1 jit_solution(15003655710527584866)
XLA Ops:
  0.0 63.3 %shard_map.145 = bf16[128,2048]{1,0:T(8,128)(2,1)S(1)} custom-call(bf16[512,256]{1,0:T(8,128)(2,1)} %value_hbm.1, bf16[512,256]{1,0:T(8,128)(2,1)} %gate_hbm_in.1, bf16[31,256]{1,0:T(8,128)(2,1)} %kernel_hbm.1, f32[1,256]{1,0:T(1,128)} %bitcast.14, f32[1,256]{1,0:T(1,128)} %bitcast.15, f32[1,256]{1,0:T(1,128)} %bitcast.16, f32[1,256]{1,0:T(1,128)} %bitcast.17, ...), custom_call_target="tpu_custom_call" | custom-call | tf_op jit(solution)/shard_map/pallas_call | solution.py:521
  63.3 0.8 %copy.17 = bf16[128,2048]{1,0:T(8,128)(2,1)} copy(bf16[128,2048]{1,0:T(8,128)(2,1)S(1)} %shard_map.145) | data formatting | bytes 1048576
